TPU v7x, 512 devices: a 4x2x32 block of a 4x8x32 slice. The times are simulated.
512 devices in a mesh: grp: 2 (over y), fs: 32 (over z), tp: 8 (over x, core).
Axes of the slice: x: 4, y: 2, z: 32, core: 2. Of those that a mesh axis runs over, the one named last changes fastest.
The devices are a block of a 4x8x32 slice.
Arguments:
- tokens: bfloat16 [64, 384, 2048], P(('grp', 'fs'), None, 'tp'), parts along dimension 0, may hold values from -24 to 24
- input_gain: float32 [2048], replicated, may hold values from 0.1 to 1.9
- query_weight: bfloat16 [2048, 1024], P('fs', 'tp'), may hold values from -0.125 to 0.125
- key_weight: bfloat16 [2048, 1024], P('fs', 'tp'), may hold values from -0.125 to 0.125
- value_weight: bfloat16 [2048, 1024], P('fs', 'tp'), may hold values from -0.125 to 0.125
- output_gate_matrix: bfloat16 [2048, 1024], P('fs', 'tp'), may hold values from -0.125 to 0.125
- forward_decay: float32 [16], P('tp'), may hold values from -1 to 9
- backward_decay: float32 [16], P('tp'), may hold values from -1 to 9
- merge_weight: bfloat16 [1024, 2048], P('tp', 'fs'), may hold values from -0.375 to 0.375
- middle_gain: float32 [2048], replicated, may hold values from 0.1 to 1.9
- gate_weight: bfloat16 [2048, 5120], P('fs', 'tp'), may hold values from -0.125 to 0.125
- up_weight: bfloat16 [2048, 5120], P('fs', 'tp'), may hold values from -0.125 to 0.125
- down_weight: bfloat16 [5120, 2048], P('tp', 'fs'), may hold values from -0.15625 to 0.15625
Outputs:
- layer_out: bfloat16 [64, 384, 2048], P(('grp', 'fs'), None, 'tp'), parts along dimension 0
There are 2 independent parts, one for each index of `grp`. A program takes and returns all parts, laid end to end along the dimension named above; an argument that names none is the same for every part. Nothing has to cross between parts.
All inputs are finite; a program needn't handle non-finite values.
Results may differ from a plain program's by a relative error of at most 0.019.
Values may be sent and summed in bfloat16 or wider, within the bound.
No kernel may reach another device: no remote copies, remote signals or barrier semaphores. Data moves between devices by JAX's collectives and lax.ppermute only.
A program may use at most 64 MiB of HBM per device.

v0:
```python
import jax
import jax.numpy as jnp
from jax import lax
from jax.sharding import PartitionSpec as P

BLOCK = 128


norm_eps = 1e-06
group_eps = 1e-05
rope_base = 10000.0
highest_precision = lax.Precision.HIGHEST


def joined_along(tiles, dim):
    tiles = jnp.moveaxis(tiles, 0, dim)
    lengths = tiles.shape
    return tiles.reshape(*lengths[:dim], lengths[dim] * lengths[dim + 1], *lengths[dim + 2 :])


def copy_for_each(array, axis):
    copies = jnp.broadcast_to(array, (lax.axis_size(axis), *array.shape))
    return lax.all_to_all(copies, axis, split_axis=0, concat_axis=0, tiled=True)


def gathered_copies(array, axis, dim):
    return joined_along(copy_for_each(array, axis), dim)


def sent_together(arrays, axis, dim, along):
    both = jnp.concatenate(arrays, axis=along)
    result, at, gathered = (lax.all_gather(both, axis, axis=dim, tiled=True), 0, [])
    for a in arrays:
        gathered.append(lax.slice_in_dim(result, at, at + a.shape[along], axis=along))
        at += a.shape[along]
    return tuple(gathered)


def split_up(array, dim, peers):
    lengths = array.shape
    tiles = array.reshape(*lengths[:dim], peers, lengths[dim] // peers, *lengths[dim + 1 :])
    return jnp.moveaxis(tiles, dim, 0)


def summed_on_arrival(array, axis, dim):
    peers = lax.axis_size(axis)
    tiles = lax.all_to_all(split_up(array, dim, peers), axis, 0, 0, tiled=True)
    return jnp.sum(tiles.astype(jnp.float32), axis=0)


def rms_scale(values, gain_vector):
    widened = values.astype(jnp.float32)
    scaled = widened * lax.rsqrt(jnp.mean(widened * widened, axis=-1, keepdims=True) + norm_eps)
    return (scaled * gain_vector).astype(jnp.bfloat16)


def apply_rotary_heads(values, length):
    half_dim = values.shape[-1] // 2
    inverse = rope_base ** (-jnp.arange(half_dim, dtype=jnp.float32) / half_dim)
    angles = jnp.arange(length, dtype=jnp.float32)[:, None] * inverse[None, :]
    cosine = jnp.cos(angles)[:, None, :]
    sine_part = jnp.sin(angles)[:, None, :]
    lower_half = values[..., :half_dim]
    upper_half = values[..., half_dim:]
    return jnp.concatenate(
        [
            lower_half * cosine - upper_half * sine_part,
            upper_half * cosine + lower_half * sine_part,
        ],
        axis=-1,
    )


def carry_states(key_blocks, value_blocks, weighting, log_rates, block_size, backward):
    block_terms = jnp.einsum(
        "sbmhd,sbmhe->bshde",
        key_blocks * weighting[None, None, :, :, None],
        value_blocks,
        precision=highest_precision,
    )
    factor = jnp.exp(log_rates * block_size)[None, :, None, None]

    def advance(running, addend):
        return (running * factor + addend, running)

    initial = jnp.zeros(block_terms.shape[1:], jnp.float32)
    return lax.scan(advance, initial, block_terms, reverse=backward)[1]


def retain_blocks(
    query_rows, key_rows, value_rows, gate_rows, forward_decay, backward_decay, seq_count, length
):
    head_count = forward_decay.shape[0]
    head_dim = query_rows.shape[1] // head_count
    block_size = BLOCK
    block_count = length // block_size

    def split_heads(rows_in):
        return rows_in.astype(jnp.float32).reshape(seq_count, length, head_count, head_dim)

    def blocked(tensor):
        return tensor.reshape(seq_count, block_count, block_size, head_count, head_dim)

    queries = blocked(apply_rotary_heads(split_heads(query_rows), length))
    key_heads = blocked(apply_rotary_heads(split_heads(key_rows), length) * head_dim ** (-0.5))
    valued = blocked(split_heads(value_rows))
    rate_ahead = jax.nn.log_sigmoid(forward_decay)
    rate_behind = jax.nn.log_sigmoid(backward_decay)
    position = jnp.arange(block_size, dtype=jnp.float32)
    offset = position[:, None] - position[None, :]
    inside = jnp.where(
        offset[None] >= 0,
        jnp.exp(rate_ahead[:, None, None] * jnp.maximum(offset, 0.0)[None]),
        jnp.exp(rate_behind[:, None, None] * jnp.maximum(-offset, 0.0)[None]),
    )
    attention_scores = (
        jnp.einsum("sbchd,sbmhd->sbhcm", queries, key_heads, precision=highest_precision)
        * inside[None, None]
    )
    result = jnp.einsum("sbhcm,sbmhd->sbchd", attention_scores, valued, precision=highest_precision)
    column = position[:, None]
    key_ahead = jnp.exp(rate_ahead[None, :] * (block_size - 1 - column))
    query_ahead = jnp.exp(rate_ahead[None, :] * (column + 1))
    key_behind = jnp.exp(rate_behind[None, :] * column)
    query_behind = jnp.exp(rate_behind[None, :] * (block_size - column))
    from_before = carry_states(key_heads, valued, key_ahead, rate_ahead, block_size, False)
    from_after = carry_states(key_heads, valued, key_behind, rate_behind, block_size, True)
    result = (
        result
        + jnp.einsum("sbchd,bshde->sbche", queries, from_before, precision=highest_precision)
        * query_ahead[None, None, :, :, None]
    )
    result = (
        result
        + jnp.einsum("sbchd,bshde->sbche", queries, from_after, precision=highest_precision)
        * query_behind[None, None, :, :, None]
    )
    result = result.reshape(seq_count, length, head_count, head_dim)
    center = jnp.mean(result, axis=-1, keepdims=True)
    spread = jnp.mean(jnp.square(result - center), axis=-1, keepdims=True)
    normalized = (result - center) * lax.rsqrt(spread + group_eps)
    gated = jax.nn.silu(split_heads(gate_rows)) * normalized
    return gated.reshape(seq_count * length, head_count * head_dim).astype(jnp.bfloat16)


def accumulate(pieces, source):
    return tuple(
        (
            jnp.dot(source, weight_piece, preferred_element_type=jnp.float32)
            for weight_piece in pieces
        )
    )


def on_device(
    tokens,
    input_gain,
    query_weight,
    key_weight,
    value_weight,
    output_gate_matrix,
    forward_decay,
    backward_decay,
    merge_weight,
    middle_gain,
    gate_weight,
    up_weight,
    down_weight,
):
    seq_count, length, part_width = tokens.shape
    row_count = seq_count * length
    gathered = gathered_copies(tokens, "tp", 2)
    normed = rms_scale(gathered.reshape(row_count, gathered.shape[2]), input_gain)
    query_sum, key_sum, value_sum, gating_sum = accumulate(
        sent_together((query_weight, key_weight, value_weight, output_gate_matrix), "fs", 0, 1),
        normed,
    )
    mixed = retain_blocks(
        query_sum.astype(jnp.bfloat16),
        key_sum.astype(jnp.bfloat16),
        value_sum.astype(jnp.bfloat16),
        gating_sum.astype(jnp.bfloat16),
        forward_decay,
        backward_decay,
        seq_count,
        length,
    )
    merge_term = jnp.dot(
        mixed,
        lax.all_gather(merge_weight, "fs", axis=1, tiled=True),
        preferred_element_type=jnp.float32,
    )
    merged = summed_on_arrival(merge_term.astype(jnp.bfloat16), "tp", 1)
    middle = (tokens.reshape(row_count, part_width).astype(jnp.float32) + merged).astype(
        jnp.bfloat16
    )
    gathered_mid = gathered_copies(middle, "tp", 1)
    normed_mid = rms_scale(gathered_mid, middle_gain)
    gate_full, up_full = sent_together((gate_weight, up_weight), "fs", 0, 1)
    gate_act = jnp.dot(normed_mid, gate_full, preferred_element_type=jnp.float32)
    up_act = jnp.dot(normed_mid, up_full, preferred_element_type=jnp.float32)
    hidden = (jax.nn.silu(gate_act) * up_act).astype(jnp.bfloat16)
    down_term = jnp.dot(
        hidden,
        lax.all_gather(down_weight, "fs", axis=1, tiled=True),
        preferred_element_type=jnp.float32,
    )
    summed = summed_on_arrival(down_term.astype(jnp.bfloat16), "tp", 1)
    layer_out = (middle.astype(jnp.float32) + summed).astype(jnp.bfloat16)
    return layer_out.reshape(seq_count, length, part_width)


def solution(mesh):
    placed = (
        P(("grp", "fs"), None, "tp"),
        P(),
        P("fs", "tp"),
        P("fs", "tp"),
        P("fs", "tp"),
        P("fs", "tp"),
        P("tp"),
        P("tp"),
        P("tp", "fs"),
        P(),
        P("fs", "tp"),
        P("fs", "tp"),
        P("tp", "fs"),
    )
    return jax.shard_map(
        on_device,
        mesh=mesh,
        in_specs=placed,
        out_specs=P(("grp", "fs"), None, "tp"),
        check_vma=False,
    )
```

profile of v0, /device:TPU:33, one launch (start us, length us, event | category | flops | bytes accessed | tf_op | source)
XLA Modules:
  0.0 478.5 jit_solution(4488102892256830335)
XLA Ops:
  6.6 1.4 pad_maximum_fusion.2
  8.1 1.6 pad_maximum_fusion.1
  9.8 1.1 copy.41
  10.9 1.3 broadcast_in_dim.28
  12.1 45.1 %all-to-all-start = ((bf16[8,1,384,256]{2,3,1,0:T(8,128)(2,1)}), bf16[8,1,384,256]{2,3,1,0:T(8,128)(2,1)S(1)}, u32[]{:S(2)}, u32[]{:S(2)}) async-start(bf16[8,1,384,256]{2,3,1,0:T(8,128)(2,1)} %broadcast_in_dim.28), calls=%async_computation | async-start | bytes 3145728 | tf_op jit(solution)/shard_map/all_to_all | solution.py:23
  57.2 0.7 all-gather.8.cloned.1.call-update
  58.3 0.3 fusion.47
  58.6 0.1 exponential_select_fusion
  58.7 51.9 %all_gather.13 = bf16[128,2048]{0,1:T(8,128)(2,1)} all-gather(bf16[128,64]{0,1:T(8,128)(2,1)S(1)} %copy-done.2), channel_id=1, replica_groups=mesh['grp'=2,'fs'=32,'tp'=8] {'fs'}, dimensions={1}, use_global_device_ids=true | all-gather | bytes 540672 | tf_op jit(solution)/shard_map/all_gather | solution.py:190
  110.6 0.4 multiply_reduce_fusion.1
  111.1 0.2 bitcast_convert_fusion
  111.3 0.5 copy-done.3
  111.8 0.4 fusion.3
  112.1 38.8 %all-gather.4.cloned.1.call-done = bf16[2048,512]{1,0:T(8,128)(2,1)} async-done(((bf16[64,512]{1,0:T(8,128)(2,1)}), bf16[2048,512]{1,0:T(8,128)(2,1)}) %all-gather.4.cloned.1.call-update) | async-done | bytes 2097168 | tf_op jit(solution)/shard_map/all_gather | solution.py:32
  150.9 1.5 convolution_convert_fusion.3
  152.5 1.5 convolution_convert_fusion.2
  154.2 1.7 convolution_convert_fusion.4
  155.9 0.1 reshape.440
  156.0 0.1 copy.47
  156.2 0.3 convolution_bitcast_fusion.4
  156.5 0.3 while.30
  156.9 0.3 convolution_bitcast_fusion.3
  157.2 0.3 while.31
  157.5 0.8 convolution_multiply_fusion
  158.3 0.5 fusion.16
  158.8 0.5 fusion.17
  159.3 0.5 fusion.56
  159.8 0.2 copy.65
  160.0 0.9 reshape.439
  161.1 0.1 copy.59
  161.2 0.1 copy.58
  161.3 3.2 convolution_convert_fusion.1
  164.5 0.1 copy.82
  164.6 46.3 %all_to_all.20 = bf16[8,384,256]{2,1,0:T(8,128)(2,1)S(1)} all-to-all(bf16[8,384,256]{2,1,0:T(8,128)(2,1)S(1)} %bitcast.140), channel_id=1, replica_groups=mesh['grp'=2,'fs'=32,'tp'=8] {'tp'}, dimensions={0} | all-to-all | bytes 3145728 | tf_op jit(solution)/shard_map/all_to_all | solution.py:47
  210.9 0.2 convert_reduce_fusion.1
  211.2 0.2 copy.61
  211.3 0.1 broadcast_in_dim.33
  211.5 24.2 %all_to_all.21 = bf16[8,384,256]{1,2,0:T(8,128)(2,1)S(1)} all-to-all(bf16[8,384,256]{1,2,0:T(8,128)(2,1)S(1)} %broadcast_in_dim.33), channel_id=1, replica_groups=mesh['grp'=2,'fs'=32,'tp'=8] {'tp'}, dimensions={0} | all-to-all | bytes 3145728 | tf_op jit(solution)/shard_map/all_to_all | solution.py:23
  235.7 0.4 multiply_reduce_fusion
  236.1 0.4 fusion.1
  236.5 52.4 %all-gather.6.cloned.1.call-done = bf16[2048,1280]{1,0:T(8,128)(2,1)} async-done(((bf16[64,1280]{1,0:T(8,128)(2,1)}), bf16[2048,1280]{1,0:T(8,128)(2,1)}) %all-gather.6.cloned.1.call-update) | async-done | bytes 5242896 | tf_op jit(solution)/shard_map/all_gather | solution.py:32
  288.9 3.2 fusion.6
  292.1 126.9 %all-gather.8.cloned.1.call-done = bf16[640,2048]{0,1:T(8,128)(2,1)} async-done(((bf16[640,64]{0,1:T(8,128)(2,1)}), bf16[640,2048]{0,1:T(8,128)(2,1)}) %all-gather.8.cloned.1.call-update) | async-done | bytes 2621456 | tf_op jit(solution)/shard_map/all_gather | solution.py:205
  419.0 6.2 %convolution_convert_fusion = bf16[384,2048]{1,0:T(8,128)(2,1)S(1)} fusion(bf16[640,2048]{0,1:T(8,128)(2,1)} %all-gather.8.cloned.1.call-done, bf16[384,2048]{0,1:T(8,128)(2,1)} %copy-done.1, bf16[2048,1280]{1,0:T(8,128)(2,1)} %all-gather.6.cloned.1.call-done, f32[384,640]{1,0:T(8,128)S(1)} %fusion.6), kind=kOutput, calls=%fused_computation.14 | convolution fusion | flops 2015526912 | bytes 9371648 | tf_op jit(solution)/shard_map/dot_general | solution.py:203
  425.1 0.1 copy.81
  425.3 45.7 %all_to_all.22 = bf16[8,384,256]{2,1,0:T(8,128)(2,1)S(1)} all-to-all(bf16[8,384,256]{2,1,0:T(8,128)(2,1)S(1)} %bitcast.141), channel_id=1, replica_groups=mesh['grp'=2,'fs'=32,'tp'=8] {'tp'}, dimensions={0} | all-to-all | bytes 3145728 | tf_op jit(solution)/shard_map/all_to_all | solution.py:47
  471.0 0.2 convert_reduce_fusion
  471.2 0.8 fusion.26
  (60 shorter events, 1.5 us)
Async XLA Ops:
  6.5 144.4 %all-gather.4.cloned.1.call-start = ((), (), s32[]{:S(2)}) async-start(), calls=%async_computation.4 | async-start | bytes 2162688 | tf_op jit(solution)/shard_map/all_gather | solution.py:32
  8.0 280.9 %all-gather.6.cloned.1.call-start = ((), (), s32[]{:S(2)}) async-start(), calls=%async_computation.5 | async-start | bytes 5406720 | tf_op jit(solution)/shard_map/all_gather | solution.py:32
  12.1 46.0 %copy-start.5 = (f32[2]{0:T(128)S(1)}, f32[2]{0:T(128)}, u32[]{:S(2)}) copy-start(f32[2]{0:T(128)} %param.24) | copy-start | bytes 28
  12.1 46.0 %copy-start.6 = (f32[2]{0:T(128)S(1)}, f32[2]{0:T(128)}, u32[]{:S(2)}) copy-start(f32[2]{0:T(128)} %param.23) | copy-start | bytes 28
  12.1 46.5 %copy-start.2 = (bf16[128,64]{0,1:T(8,128)(2,1)S(1)}, bf16[128,64]{0,1:T(8,128)(2,1)}, u32[]{:S(2)}) copy-start(bf16[128,64]{0,1:T(8,128)(2,1)} %param.25) | copy-start | bytes 49156
  12.1 98.5 %all-to-all-start = ((bf16[8,1,384,256]{2,3,1,0:T(8,128)(2,1)}), bf16[8,1,384,256]{2,3,1,0:T(8,128)(2,1)S(1)}, u32[]{:S(2)}, u32[]{:S(2)}) async-start(bf16[8,1,384,256]{2,3,1,0:T(8,128)(2,1)} %broadcast_in_dim.28), calls=%async_computation | async-start | bytes 3145728 | tf_op jit(solution)/shard_map/all_to_all | solution.py:23
  57.2 361.8 %all-gather.8.cloned.1.call-start = ((), (), s32[]{:S(2)}) async-start(), calls=%async_computation.6 | async-start | bytes 2703360 | tf_op jit(solution)/shard_map/all_gather | solution.py:205
  111.1 0.7 copy-start.3
  164.6 46.5 %copy-start = (bf16[1,384,256]{2,1,0:T(8,128)(2,1)S(1)}, bf16[1,384,256]{2,1,0:T(8,128)(2,1)}, u32[]{:S(2)}) copy-start(bf16[1,384,256]{2,1,0:T(8,128)(2,1)} %param.17) | copy-start | bytes 589828
  211.5 24.6 %copy-start.4 = (f32[2048]{0:T(1024)S(1)}, f32[2048]{0:T(1024)}, u32[]{:S(2)}) copy-start(f32[2048]{0:T(1024)} %param.26) | copy-start | bytes 24580
  236.5 55.6 %copy-start.1 = (bf16[384,2048]{0,1:T(8,128)(2,1)}, bf16[384,2048]{0,1:T(8,128)(2,1)S(1)}, u32[]{:S(2)}) copy-start(bf16[384,2048]{0,1:T(8,128)(2,1)S(1)} %fusion.1) | copy-start | bytes 4718596
Sparse Core Ops, SparseCore 0:
  9.4 141.4 all-gather.3
  153.0 135.8 all-gather.5
  291.0 127.9 all-gather.7
where the time goes:
time: 479 us
  waiting for transfers between devices  219 us (46%)
  blocking collectives  168 us (35%)
  starting transfers between devices  45.1 us (9%)
  matrix products  20.1 us (4%)
  between operations  13.6 us (3%)
  other arithmetic  7.42 us (2%)
  local copies, waits for them, and re-layouts  5.26 us (1%)
    all_gather x1, waiting for transfers between devices, on_device(): lax.all_gather(down_weight, 'fs', axis=1, tiled=True)  127 us
    all_to_all x2, blocking collectives, summed_on_arrival(): tiles = lax.all_to_all(split_up(array, dim, peers), axis, 0, 0, tiled=True)  92 us
    all_gather x2, waiting for transfers between devices, sent_together(): lax.all_gather(both, axis, axis=dim, tiled=True)  91.2 us
    all_gather x1, blocking collectives, on_device(): lax.all_gather(merge_weight, 'fs', axis=1, tiled=True)  51.9 us
    all_to_all x1, starting transfers between devices, copy_for_each(): return lax.all_to_all(copies, axis, split_axis=0, concat_axis=0, tiled=True)  45.1 us
    all_to_all x1, blocking collectives, copy_for_each(): return lax.all_to_all(copies, axis, split_axis=0, concat_axis=0, tiled=True)  24.2 us
  transfers between devices with their start and end apart: 4, of which 3 were waited for; matrix products, arithmetic and copies ran while one was open for 5% of the time, Pallas kernels for 0%

commit v1 on v0

--- a/solution.py
+++ b/solution.py
@@ -12,39 +12,33 @@
 highest_precision = lax.Precision.HIGHEST
 
 
-def joined_along(tiles, dim):
-    tiles = jnp.moveaxis(tiles, 0, dim)
-    lengths = tiles.shape
-    return tiles.reshape(*lengths[:dim], lengths[dim] * lengths[dim + 1], *lengths[dim + 2 :])
-
-
-def copy_for_each(array, axis):
-    copies = jnp.broadcast_to(array, (lax.axis_size(axis), *array.shape))
-    return lax.all_to_all(copies, axis, split_axis=0, concat_axis=0, tiled=True)
-
-
-def gathered_copies(array, axis, dim):
-    return joined_along(copy_for_each(array, axis), dim)
-
-
-def sent_together(arrays, axis, dim, along):
-    both = jnp.concatenate(arrays, axis=along)
-    result, at, gathered = (lax.all_gather(both, axis, axis=dim, tiled=True), 0, [])
-    for a in arrays:
-        gathered.append(lax.slice_in_dim(result, at, at + a.shape[along], axis=along))
-        at += a.shape[along]
-    return tuple(gathered)
-
-
-def split_up(array, dim, peers):
-    lengths = array.shape
-    tiles = array.reshape(*lengths[:dim], peers, lengths[dim] // peers, *lengths[dim + 1 :])
-    return jnp.moveaxis(tiles, dim, 0)
-
-
-def summed_on_arrival(array, axis, dim):
-    peers = lax.axis_size(axis)
-    tiles = lax.all_to_all(split_up(array, dim, peers), axis, 0, 0, tiled=True)
+def core_pairs():
+    peers = lax.axis_size("tp")
+    return [[i, i + 1] for i in range(0, peers, 2)]
+
+
+def chip_rings():
+    peers = lax.axis_size("tp")
+    return [list(range(0, peers, 2)), list(range(1, peers, 2))]
+
+
+def gathered_features(shard):
+    chips = lax.all_gather(shard, "tp", axis=0, axis_index_groups=chip_rings())
+    both = jnp.broadcast_to(chips, (2, *chips.shape))
+    both = lax.all_to_all(both, "tp", 0, 0, tiled=True, axis_index_groups=core_pairs())
+    return jnp.concatenate(
+        [both[c, x] for x in range(chips.shape[0]) for c in range(2)], axis=1
+    )
+
+
+def scattered_sum(partial_term):
+    peers = lax.axis_size("tp")
+    rows, width = partial_term.shape[0], partial_term.shape[1] // peers
+    parts = [partial_term[:, t * width : (t + 1) * width] for t in range(peers)]
+    tiles = jnp.stack([jnp.stack(parts[0::2]), jnp.stack(parts[1::2])])
+    tiles = lax.all_to_all(tiles, "tp", 0, 0, tiled=True, axis_index_groups=core_pairs())
+    chip_sum = (tiles[0].astype(jnp.float32) + tiles[1].astype(jnp.float32)).astype(jnp.bfloat16)
+    tiles = lax.all_to_all(chip_sum, "tp", 0, 0, tiled=True, axis_index_groups=chip_rings())
     return jnp.sum(tiles.astype(jnp.float32), axis=0)
 
 
@@ -141,15 +135,6 @@
     normalized = (result - center) * lax.rsqrt(spread + group_eps)
     gated = jax.nn.silu(split_heads(gate_rows)) * normalized
     return gated.reshape(seq_count * length, head_count * head_dim).astype(jnp.bfloat16)
-
-
-def accumulate(pieces, source):
-    return tuple(
-        (
-            jnp.dot(source, weight_piece, preferred_element_type=jnp.float32)
-            for weight_piece in pieces
-        )
-    )
 
 
 def on_device(
@@ -169,43 +154,48 @@
 ):
     seq_count, length, part_width = tokens.shape
     row_count = seq_count * length
-    gathered = gathered_copies(tokens, "tp", 2)
-    normed = rms_scale(gathered.reshape(row_count, gathered.shape[2]), input_gain)
-    query_sum, key_sum, value_sum, gating_sum = accumulate(
-        sent_together((query_weight, key_weight, value_weight, output_gate_matrix), "fs", 0, 1),
-        normed,
-    )
+    pieces = (
+        query_weight,
+        key_weight,
+        value_weight,
+        output_gate_matrix,
+        merge_weight.T,
+        gate_weight,
+        up_weight,
+        down_weight.T,
+    )
+    packed = lax.all_gather(jnp.concatenate(pieces, axis=1), "fs", axis=0, tiled=True)
+    full, at = [], 0
+    for piece in pieces:
+        full.append(packed[:, at : at + piece.shape[1]])
+        at += piece.shape[1]
+    query_full, key_full, value_full, gating_full, merge_full, gate_full, up_full, down_full = full
+
+    local = tokens.reshape(row_count, part_width)
+    normed = rms_scale(gathered_features(local), input_gain)
+
+    def project(weight):
+        return jnp.dot(normed, weight, preferred_element_type=jnp.float32).astype(jnp.bfloat16)
+
     mixed = retain_blocks(
-        query_sum.astype(jnp.bfloat16),
-        key_sum.astype(jnp.bfloat16),
-        value_sum.astype(jnp.bfloat16),
-        gating_sum.astype(jnp.bfloat16),
+        project(query_full),
+        project(key_full),
+        project(value_full),
+        project(gating_full),
         forward_decay,
         backward_decay,
         seq_count,
         length,
     )
-    merge_term = jnp.dot(
-        mixed,
-        lax.all_gather(merge_weight, "fs", axis=1, tiled=True),
-        preferred_element_type=jnp.float32,
-    )
-    merged = summed_on_arrival(merge_term.astype(jnp.bfloat16), "tp", 1)
-    middle = (tokens.reshape(row_count, part_width).astype(jnp.float32) + merged).astype(
-        jnp.bfloat16
-    )
-    gathered_mid = gathered_copies(middle, "tp", 1)
-    normed_mid = rms_scale(gathered_mid, middle_gain)
-    gate_full, up_full = sent_together((gate_weight, up_weight), "fs", 0, 1)
+    merge_term = jnp.einsum("rh,dh->rd", mixed, merge_full, preferred_element_type=jnp.float32)
+    merged = scattered_sum(merge_term.astype(jnp.bfloat16))
+    middle = (local.astype(jnp.float32) + merged).astype(jnp.bfloat16)
+    normed_mid = rms_scale(gathered_features(middle), middle_gain)
     gate_act = jnp.dot(normed_mid, gate_full, preferred_element_type=jnp.float32)
     up_act = jnp.dot(normed_mid, up_full, preferred_element_type=jnp.float32)
     hidden = (jax.nn.silu(gate_act) * up_act).astype(jnp.bfloat16)
-    down_term = jnp.dot(
-        hidden,
-        lax.all_gather(down_weight, "fs", axis=1, tiled=True),
-        preferred_element_type=jnp.float32,
-    )
-    summed = summed_on_arrival(down_term.astype(jnp.bfloat16), "tp", 1)
+    down_term = jnp.einsum("rh,dh->rd", hidden, down_full, preferred_element_type=jnp.float32)
+    summed = scattered_sum(down_term.astype(jnp.bfloat16))
     layer_out = (middle.astype(jnp.float32) + summed).astype(jnp.bfloat16)
     return layer_out.reshape(seq_count, length, part_width)
 

time: 479 us -> 291 us (0.61)
  waiting for transfers between devices: 219 us -> 104 us
  blocking collectives: 168 us -> 88.4 us
  local copies, waits for them, and re-layouts: 5.26 us -> 11.1 us
    all_gather x3 -> x1, waiting for transfers between devices: 218 us -> 102 us  [on_device(): lax.all_gather(jnp.concatenate(pieces, axis=1), 'fs', axis=0, tiled=True)]
    all_to_all x3 -> x5, blocking collectives: 116 us -> 64.7 us  [the longest x2 29.6 us: scattered_sum(): lax.all_to_all(chip_sum, 'tp', 0, 0, tiled=True, axis_index_groups=chip_r...]
    all_gather x1 -> x2, blocking collectives: 51.9 us -> 23.8 us  [gathered_features(): chips = lax.all_gather(shard, 'tp', axis=0, axis_index_groups=chip_rings())]
    unnamed x15 -> x34, local copies, waits for them, and re-layouts: 0.51 us -> 6.77 us
  transfers between devices with their start and end apart: 4 -> 2, of which waited for: 3 -> 2; matrix products, arithmetic and copies ran while one was open for 5% -> 1% of each run, Pallas kernels for 0% -> 0%
where the time goes in v1:
time: 291 us; the launch traced here: 290 us
  waiting for transfers between devices  104 us (36%)
  blocking collectives  88.4 us (30%)
  starting transfers between devices  46.6 us (16%)
  matrix products  20.9 us (7%)
  between operations  14 us (5%)
  local copies, waits for them, and re-layouts  11.1 us (4%)
  other arithmetic  4.59 us (2%)
    all_gather x1, waiting for transfers between devices, on_device(): lax.all_gather(jnp.concatenate(pieces, axis=1), 'fs', axis=0, tiled=True)  102 us
    all_to_all x1, starting transfers between devices, gathered_features(): lax.all_to_all(both, 'tp', 0, 0, tiled=True, axis_index_groups=core_pairs())  46.6 us
    all_to_all x2, blocking collectives, scattered_sum(): lax.all_to_all(chip_sum, 'tp', 0, 0, tiled=True, axis_index_groups=chip_r...  29.6 us
    all_to_all x2, blocking collectives, scattered_sum(): lax.all_to_all(tiles, 'tp', 0, 0, tiled=True, axis_index_groups=core_pair...  26 us
    all_gather x2, blocking collectives, gathered_features(): chips = lax.all_gather(shard, 'tp', axis=0, axis_index_groups=chip_rings())  23.8 us
    all_to_all x1, blocking collectives, gathered_features(): lax.all_to_all(both, 'tp', 0, 0, tiled=True, axis_index_groups=core_pairs())  9.1 us
    unnamed x34, local copies, waits for them, and re-layouts  6.77 us
    dot_general x1, matrix products, on_device(): jnp.einsum('rh,dh->rd', hidden, down_full, preferred_element_type=jnp.flo...  5.93 us
  transfers between devices with their start and end apart: 2, of which 2 were waited for; matrix products, arithmetic and copies ran while one was open for 1% of the time, Pallas kernels for 0%

profile of v1, /device:TPU:33, one launch (start us, length us, event | category | flops | bytes accessed | tf_op | source)
XLA Modules:
  0.0 289.6 jit_solution(2907152177668310477)
XLA Ops:
  6.6 0.7 constant_dynamic-update-slice_fusion.6
  7.3 0.7 constant_dynamic-update-slice_fusion.5
  8.0 0.7 constant_dynamic-update-slice_fusion.4
  8.7 0.7 constant_dynamic-update-slice_fusion.3
  9.4 0.7 constant_dynamic-update-slice_fusion.2
  10.2 0.9 constant_dynamic-update-slice_fusion.1
  11.1 0.9 constant_dynamic-update-slice_fusion
  12.0 0.9 bitcast_dynamic-update-slice_fusion.2
  12.9 0.7 copy-done.1
  13.7 12.1 %all_gather.10 = bf16[4,384,256]{2,1,0:T(8,128)(2,1)S(1)} all-gather(bf16[1,384,256]{2,1,0:T(8,128)(2,1)} %param.17), channel_id=1, replica_groups={{0,2,4,6},{1,3,5,7},{8,10,12,14},{9,11,13,15},{16,18,20,22},{17,19,21,2..., dimensions={0}, use_global_device_ids=true | all-gather | bytes 983040 | tf_op jit(solution)/shard_map/all_gather | solution.py:26
  25.8 1.2 broadcast_in_dim.28
  27.0 46.6 %all-to-all-start = ((bf16[2,4,384,256]{3,2,1,0:T(8,128)(2,1)}), bf16[2,4,384,256]{3,2,1,0:T(8,128)(2,1)S(1)}, u32[]{:S(2)}, u32[]{:S(2)}) async-start(bf16[2,4,384,256]{3,2,1,0:T(8,128)(2,1)} %broadcast_in_dim.28), calls=%async_computation | async-start | bytes 3145728 | tf_op jit(solution)/shard_map/all_to_all | solution.py:28
  73.7 2.0 all-to-all-done
  76.0 0.4 fusion
  76.3 0.1 copy-done.3
  76.7 0.3 fusion.75
  77.1 0.4 fusion.2
  77.5 101.9 %all-gather.2.cloned.1.call-done = bf16[2048,2560]{1,0:T(8,128)(2,1)} async-done(((bf16[64,2560]{1,0:T(8,128)(2,1)}), bf16[2048,2560]{1,0:T(8,128)(2,1)}) %all-gather.2.cloned.1.call-update) | async-done | bytes 10485776 | tf_op jit(solution)/shard_map/all_gather | solution.py:167
  179.4 1.6 convolution_convert_fusion.2
  181.0 1.6 convolution_convert_fusion.3
  183.0 1.6 convolution_convert_fusion.4
  184.7 0.1 copy.60
  184.9 0.3 convolution_bitcast_fusion.4
  185.2 0.3 while.30
  185.5 0.3 convolution_bitcast_fusion.3
  185.8 0.3 while.31
  186.1 0.8 convolution_multiply_fusion
  186.9 0.5 fusion.19
  187.4 0.5 fusion.20
  187.9 0.5 fusion.84
  188.4 0.2 copy.75
  188.6 0.9 reshape.432
  189.9 3.1 %convolution_convert_fusion.1 = bf16[384,2048]{1,0:T(8,128)(2,1)S(1)} fusion(bf16[2048,2560]{1,0:T(8,128)(2,1)} %all-gather.2.cloned.1.call-done, f32[384,128]{1,0:T(8,128)S(1)} %copy.72, f32[384,128]{1,0:T(8,128)} %reshape.432, f32[384,128]{1,0:T(8,128)S(1)} %copy.71, bf16[384,2048]{1,0:T(8,128)(2,1)S(1)} %fusion.2), kind=kOutput, calls=%fused_computation.15 | convolution fusion | flops 403931136 | bytes 4784128 | tf_op jit(solution)/shard_map/rh,dh->rd/dot_general | solution.py:190
  193.4 0.1 pad_maximum_fusion
  193.6 21.0 %all_to_all.30 = bf16[2,4,384,256]{3,2,1,0:T(8,128)(2,1)S(1)} all-to-all(bf16[2,4,384,256]{3,2,1,0:T(8,128)(2,1)S(1)} %pad_maximum_fusion), channel_id=1, replica_groups={{0,1},{2,3},{4,5},{6,7},{8,9},{10,11},{12,13},{14,15},{16,17},{18,19},{..., dimensions={0} | all-to-all | bytes 3145728 | tf_op jit(solution)/shard_map/all_to_all | solution.py:39
  214.6 0.2 fusion.27
  214.8 15.2 %all_to_all.31 = bf16[4,384,256]{2,1,0:T(8,128)(2,1)S(1)} all-to-all(bf16[4,384,256]{2,1,0:T(8,128)(2,1)S(1)} %fusion.27), channel_id=1, replica_groups={{0,2,4,6},{1,3,5,7},{8,10,12,14},{9,11,13,15},{16,18,20,22},{17,19,21,2..., dimensions={0} | all-to-all | bytes 1572864 | tf_op jit(solution)/shard_map/all_to_all | solution.py:41
  230.2 11.6 %all_gather.12 = bf16[4,384,256]{2,1,0:T(8,128)(2,1)S(1)} all-gather(bf16[1,384,256]{2,1,0:T(8,128)(2,1)S(1)} %fusion.39), channel_id=1, replica_groups={{0,2,4,6},{1,3,5,7},{8,10,12,14},{9,11,13,15},{16,18,20,22},{17,19,21,2..., dimensions={0}, use_global_device_ids=true | all-gather | bytes 983040 | tf_op jit(solution)/shard_map/all_gather | solution.py:26
  242.0 9.1 %all_to_all.32 = bf16[2,4,384,256]{3,2,1,0:T(8,128)(2,1)S(1)} all-to-all(bf16[2,4,384,256]{3,2,1,0:T(8,128)(2,1)S(1)} %broadcast_in_dim.33), channel_id=1, replica_groups={{0,1},{2,3},{4,5},{6,7},{8,9},{10,11},{12,13},{14,15},{16,17},{18,19},{..., dimensions={0} | all-to-all | bytes 3145728 | tf_op jit(solution)/shard_map/all_to_all | solution.py:28
  251.3 0.4 fusion.3
  251.7 0.2 copy-done.5
  251.9 4.1 %fusion.9 = f32[384,640]{1,0:T(8,128)} fusion(bf16[2048,2560]{1,0:T(8,128)(2,1)} %all-gather.2.cloned.1.call-done, bf16[384,2048]{1,0:T(8,128)(2,1)S(1)} %fusion.40, f32[2048]{0:T(1024)S(1)} %copy-done.5, f32[384]{0:T(512)S(1)} %add_rsqrt_fusion), kind=kOutput, calls=%fused_computation.19 | convolution fusion | flops 1009778688 | bytes 5187072 | tf_op jit(solution)/shard_map/dot_general | solution.py:194
  256.0 5.9 %convolution_convert_fusion = bf16[384,2048]{1,0:T(8,128)(2,1)S(1)} fusion(bf16[2048,2560]{1,0:T(8,128)(2,1)} %all-gather.2.cloned.1.call-done, f32[384,640]{1,0:T(8,128)} %fusion.9, bf16[384,2048]{1,0:T(8,128)(2,1)S(1)} %fusion.40, f32[2048]{0:T(1024)S(1)} %copy-done.5, f32[384]{0:T(512)S(1)} %add_rsqrt_fusion), kind=kOutput, calls=%fused_computation.14 | convolution fusion | flops 2018672640 | bytes 9381376 | tf_op jit(solution)/shard_map/rh,dh->rd/dot_general | solution.py:197
  262.3 0.1 pad_maximum_fusion.1
  262.4 4.9 %all_to_all.33 = bf16[2,4,384,256]{3,2,1,0:T(8,128)(2,1)S(1)} all-to-all(bf16[2,4,384,256]{3,2,1,0:T(8,128)(2,1)S(1)} %pad_maximum_fusion.1), channel_id=1, replica_groups={{0,1},{2,3},{4,5},{6,7},{8,9},{10,11},{12,13},{14,15},{16,17},{18,19},{..., dimensions={0} | all-to-all | bytes 3145728 | tf_op jit(solution)/shard_map/all_to_all | solution.py:39
  267.4 0.2 fusion.28
  267.6 14.3 %all_to_all.34 = bf16[4,384,256]{2,1,0:T(8,128)(2,1)S(1)} all-to-all(bf16[4,384,256]{2,1,0:T(8,128)(2,1)S(1)} %fusion.28), channel_id=1, replica_groups={{0,2,4,6},{1,3,5,7},{8,10,12,14},{9,11,13,15},{16,18,20,22},{17,19,21,2..., dimensions={0} | all-to-all | bytes 1572864 | tf_op jit(solution)/shard_map/all_to_all | solution.py:41
  282.0 0.7 fusion.38
  (81 shorter events, 3.0 us)
Async XLA Ops:
  6.5 172.9 %all-gather.2.cloned.1.call-start = ((), (), s32[]{:S(2)}) async-start(), calls=%async_computation.6 | async-start | bytes 10813440 | tf_op jit(solution)/shard_map/all_gather | solution.py:167
  12.9 0.7 copy-start.1
  27.0 48.7 %all-to-all-start = ((bf16[2,4,384,256]{3,2,1,0:T(8,128)(2,1)}), bf16[2,4,384,256]{3,2,1,0:T(8,128)(2,1)S(1)}, u32[]{:S(2)}, u32[]{:S(2)}) async-start(bf16[2,4,384,256]{3,2,1,0:T(8,128)(2,1)} %broadcast_in_dim.28), calls=%async_computation | async-start | bytes 3145728 | tf_op jit(solution)/shard_map/all_to_all | solution.py:28
  75.8 0.7 copy-start.3
  75.8 0.7 copy-start.4
  75.9 1.2 copy-start.2
  214.8 15.4 %copy-start = (bf16[1,384,256]{2,1,0:T(8,128)(2,1)S(1)}, bf16[1,384,256]{2,1,0:T(8,128)(2,1)}, u32[]{:S(2)}) copy-start(bf16[1,384,256]{2,1,0:T(8,128)(2,1)} %param.17) | copy-start | bytes 589828
  251.2 0.7 copy-start.5
Sparse Core Ops, SparseCore 0:
  13.8 165.5 all-gather.1
